TPU v7x, 32 devices: a whole 2x2x4 slice. The times are simulated.
32 devices in a mesh: ep: 8 (over z, x), tp: 4 (over y, core).
Axes of the slice: x: 2, y: 2, z: 4, core: 2. Of those that a mesh axis runs over, the one named last changes fastest.
Arguments:
- hidden: bfloat16 [256, 4096], P('ep', 'tp'), may hold values from -6 to 6
- norm_gain: float32 [4096], P('tp'), may hold values from 0.1 to 1.9
- expert_ids: int32 [256, 8], P('ep'), may hold values from 0 to 15, as said below
- route_weights: float32 [256, 8], P('ep'), may hold values from 0.1 to 1
- lengths: int32 [32], P('ep'), may hold values from 1 to 8, as said below
- gate_proj: bfloat16 [16, 4096, 1024], P('ep', None, 'tp'), may hold values from -0.09375 to 0.09375
- up_proj: bfloat16 [16, 4096, 1024], P('ep', None, 'tp'), may hold values from -0.09375 to 0.09375
- down_proj: bfloat16 [16, 1024, 4096], P('ep', 'tp'), may hold values from -0.1875 to 0.1875
- shared_gate: bfloat16 [4096, 1024], P(None, 'tp'), may hold values from -0.09375 to 0.09375
- shared_up: bfloat16 [4096, 1024], P(None, 'tp'), may hold values from -0.09375 to 0.09375
- shared_down: bfloat16 [1024, 4096], P('tp'), may hold values from -0.1875 to 0.1875
Outputs:
- mixed: bfloat16 [256, 4096], P('ep', 'tp')
Inputs may be any that keep to these rules, and one draw needn't show every extreme that they name: `expert_ids`: among the 32 rows of one index of ep (an aligned block), no expert is named more than 32 times, and in every block one expert is named exactly 32 times; each row names 8 different experts. `lengths`: each sequence has 1 to 8 live slots; on some index of ep all 4 sequences have 8 live slots.
All inputs are finite; a program needn't handle non-finite values.
Results may differ from a plain program's by a relative error of at most 0.015.
Values may be sent and summed in bfloat16 or wider, within the bound.
A program may use at most 128 MiB of HBM per device.

v0:
```python
import jax
import jax.numpy as jnp
from jax import lax
from jax.sharding import PartitionSpec as P

epsilon = 1e-06


def gathered_experts(source_rows, expert_ids, mixing, gate_proj, up_proj, down_proj, expert_count):
    local_experts = gate_proj.shape[0]
    is_named = expert_ids[:, :, None] == jnp.arange(expert_count, dtype=jnp.int32)[None, None, :]
    by_expert = jnp.sum(jnp.where(is_named, mixing[:, :, None], 0.0), axis=1)
    gathered_rows = lax.all_gather(source_rows, "ep", axis=0, tiled=True)
    all_rows = gathered_rows[None, None][0, 0]
    all_weights = lax.all_gather(by_expert, "ep", axis=0, tiled=True)
    first_expert = lax.axis_index("ep") * local_experts
    weight_block = all_weights
    weight_block = lax.dynamic_slice_in_dim(weight_block, first_expert, local_experts, 1)
    gate_value = jnp.einsum("rd,edf->erf", all_rows, gate_proj, preferred_element_type=jnp.float32)
    up_value = jnp.einsum("rd,edf->erf", all_rows, up_proj, preferred_element_type=jnp.float32)
    inner_value = (jax.nn.silu(gate_value) * up_value).astype(jnp.bfloat16)
    result = jnp.einsum("erf,efd->erd", inner_value, down_proj, preferred_element_type=jnp.float32)
    return lax.psum_scatter(
        jnp.sum(weight_block.T[:, :, None] * result, axis=0).astype(jnp.bfloat16),
        "ep",
        scatter_dimension=0,
        tiled=True,
    ).astype(jnp.float32)


def body(
    hidden,
    norm_gain,
    expert_ids,
    route_weights,
    lengths,
    gate_proj,
    up_proj,
    down_proj,
    shared_gate,
    shared_up,
    shared_down,
):
    slot_count = hidden.shape[0]
    span_size = slot_count // lengths.shape[0]
    local_experts = gate_proj.shape[0]
    expert_count = local_experts * lax.axis_size("ep")
    model_width = hidden.shape[1] * lax.axis_size("tp")
    values = hidden.astype(jnp.float32)
    squares = lax.psum(jnp.sum(values * values, axis=1), "tp")
    row_scale = lax.rsqrt(squares / model_width + epsilon)
    normed = (values * row_scale[:, None] * norm_gain[None, :]).astype(jnp.bfloat16)
    full_rows = lax.all_gather(normed, "tp", axis=1, tiled=True)
    offsets = jnp.arange(slot_count, dtype=jnp.int32) % span_size
    is_live = offsets < jnp.repeat(lengths, span_size)
    mixing = jnp.where(is_live[:, None], route_weights, 0.0)
    shared_inner = (
        jax.nn.silu(jnp.dot(full_rows, shared_gate, preferred_element_type=jnp.float32))
        * jnp.dot(full_rows, shared_up, preferred_element_type=jnp.float32)
    ).astype(jnp.bfloat16)
    shared_part = jnp.dot(shared_inner, shared_down, preferred_element_type=jnp.float32)
    routed = gathered_experts(
        full_rows, expert_ids, mixing, gate_proj, up_proj, down_proj, expert_count
    )
    combined = lax.psum_scatter(
        (routed + shared_part).astype(jnp.bfloat16), "tp", scatter_dimension=1, tiled=True
    ).astype(jnp.float32)
    return jnp.where(is_live[:, None], combined, 0.0).astype(jnp.bfloat16)


def solution(mesh):
    placed = (
        P("ep", "tp"),
        P("tp"),
        P("ep", None),
        P("ep", None),
        P("ep"),
        P("ep", None, "tp"),
        P("ep", None, "tp"),
        P("ep", "tp", None),
        P(None, "tp"),
        P(None, "tp"),
        P("tp", None),
    )
    return jax.shard_map(body, mesh=mesh, in_specs=placed, out_specs=P("ep", "tp"), check_vma=False)
```

profile of v0, /device:TPU:0, one launch (start us, length us, event | category | flops | bytes accessed | tf_op | source)
XLA Modules:
  0.0 184.0 jit_solution(5941911007509637524)
XLA Ops:
  6.5 1.1 fusion.26
  7.6 8.4 %psum.7 = f32[32]{0:T(128)S(1)} all-reduce(f32[32]{0:T(128)S(1)} %fusion.26), channel_id=1, replica_groups=mesh['ep'=8,'tp'=4] {'tp'}, use_global_device_ids=true, to_apply=%region_2.3 | all-reduce | flops 32 | bytes 256 | tf_op jit(solution)/shard_map/psum | solution.py:50
  16.1 0.9 fusion.28
  17.0 6.2 %all_gather.10 = bf16[32,4096]{1,0:T(8,128)(2,1)} all-gather(bf16[32,1024]{1,0:T(8,128)(2,1)S(1)} %fusion.28), channel_id=1, replica_groups=mesh['ep'=8,'tp'=4] {'tp'}, dimensions={1}, use_global_device_ids=true | all-gather | bytes 327680 | tf_op jit(solution)/shard_map/all_gather | solution.py:53
  23.2 0.0 all-gather.3.cloned.1.call-update
  23.2 0.0 reduce-scatter.3.cloned.1.call-start
  23.3 0.7 broadcast_in_dim.47
  24.0 0.1 reshape.22
  24.1 0.7 broadcast_select_fusion
  24.8 0.7 select_reduce_fusion
  25.5 31.2 %all-gather = f32[8,32,16]{1,2,0:T(8,128)S(1)} all-gather(f32[1,32,16]{1,2,0:T(8,128)S(1)} %bitcast.38), channel_id=1, replica_groups=mesh['ep'=8,'tp'=4] {'ep'}, dimensions={0}, use_global_device_ids=true | all-gather | bytes 18432 | tf_op jit(solution)/shard_map/all_gather | solution.py:15
  56.7 0.1 reshape.24
  56.8 16.0 %all-gather.3.cloned.1.call-done = bf16[256,4096]{1,0:T(8,128)(2,1)} async-done(((bf16[32,4096]{1,0:T(8,128)(2,1)}), bf16[256,4096]{1,0:T(8,128)(2,1)}) %all-gather.3.cloned.1.call-update) | async-done | bytes 2097168 | tf_op jit(solution)/shard_map/all_gather | solution.py:13
  72.8 4.1 %fusion.5 = f32[2,256,256]{2,1,0:T(8,128)S(1)} fusion(bf16[2,4096,256]{2,1,0:T(8,128)(2,1)} %param.16, bf16[256,4096]{1,0:T(8,128)(2,1)} %all-gather.3.cloned.1.call-done), kind=kOutput, calls=%fused_computation.7 | convolution fusion | flops 1073741824 | bytes 6815744 | tf_op jit(solution)/shard_map/rd,edf->erf/dot_general | solution.py:19
  76.9 8.6 %multiply_reduce_fusion = bf16[256,4096]{1,0:T(8,128)(2,1)} fusion(bf16[2,256,4096]{2,1,0:T(8,128)(2,1)} %param.18, f32[2,256]{1,0:T(2,128)S(1)} %dynamic-slice_bitcast_fusion, bf16[2,4096,256]{2,1,0:T(8,128)(2,1)} %param.17, bf16[256,4096]{1,0:T(8,128)(2,1)} %all-gather.3.cloned.1.call-done, f32[2,256,256]{2,1,0:T(8,128)S(1)} %fusion.5), kind=kOutput, calls=%fused_computation | convolution fusion | flops 2151415808 | bytes 13109248 | tf_op jit(solution)/shard_map/erf,efd->erd/dot_general | solution.py:22
  85.5 0.0 reduce-scatter.3.cloned.1.call-update
  85.5 0.0 reduce-scatter.5.cloned.1.call-start
  85.6 0.9 copy-done.1
  86.4 2.0 %fusion.38 = f32[32,256]{1,0:T(8,128)S(1)} fusion(bf16[32,4096]{1,0:T(8,128)(2,1)S(1)} %copy-done.1, bf16[4096,256]{1,0:T(8,128)(2,1)} %param.19), kind=kOutput, calls=%fused_computation.40 | convolution fusion | flops 67108864 | bytes 2392064 | tf_op jit(solution)/shard_map/dot_general | solution.py:58
  88.5 64.6 %reduce-scatter.3.cloned.1.call-done = bf16[32,4096]{1,0:T(8,128)(2,1)} async-done(((bf16[256,4096]{1,0:T(8,128)(2,1)}), bf16[32,4096]{1,0:T(8,128)(2,1)}) %reduce-scatter.3.cloned.1.call-update) | async-done | bytes 262160 | tf_op jit(solution)/shard_map/reduce_scatter | solution.py:23
  153.1 3.6 %fusion = bf16[32,4096]{1,0:T(8,128)(2,1)} fusion(bf16[256,4096]{1,0:T(8,128)(2,1)S(1)} %copy-done, bf16[32,4096]{1,0:T(8,128)(2,1)S(1)} %copy-done.1, bf16[4096,256]{1,0:T(8,128)(2,1)} %param.20, bf16[32,4096]{1,0:T(8,128)(2,1)} %reduce-scatter.3.cloned.1.call-done, f32[32,256]{1,0:T(8,128)S(1)} %fusion.38), kind=kOutput, calls=%fused_computation.2 | convolution fusion | flops 134660096 | bytes 5013504 | tf_op jit(solution)/shard_map/dot_general | solution.py:61
  156.7 0.0 reduce-scatter.5.cloned.1.call-update
  156.7 19.2 %reduce-scatter.5.cloned.1.call-done = bf16[32,1024]{1,0:T(8,128)(2,1)} async-done(((bf16[32,4096]{1,0:T(8,128)(2,1)}), bf16[32,1024]{1,0:T(8,128)(2,1)}) %reduce-scatter.5.cloned.1.call-update) | async-done | bytes 65552 | tf_op jit(solution)/shard_map/reduce_scatter | solution.py:65
  175.9 1.5 select_convert_fusion
  (8 shorter events, 0.1 us)
Async XLA Ops:
  6.5 146.6 %copy-start = (bf16[256,4096]{1,0:T(8,128)(2,1)S(1)}, bf16[256,4096]{1,0:T(8,128)(2,1)}, u32[]{:S(2)}) copy-start(bf16[256,4096]{1,0:T(8,128)(2,1)} %param.21) | copy-start | bytes 6291460
  6.5 66.3 %all-gather.3.cloned.1.call-start = ((), (), s32[]{:S(2)}) async-start(), calls=%async_computation.2 | async-start | bytes 2359296 | tf_op jit(solution)/shard_map/all_gather | solution.py:13
  23.2 129.9 %reduce-scatter.3.cloned.1.call-start = ((), (), s32[]{:S(2)}) async-start(), calls=%async_computation.3 | async-start | bytes 2359296 | tf_op jit(solution)/shard_map/reduce_scatter | solution.py:23
  85.5 0.9 copy-start.1
  85.5 90.4 %reduce-scatter.5.cloned.1.call-start = ((), (), s32[]{:S(2)}) async-start(), calls=%async_computation.4 | async-start | bytes 327680 | tf_op jit(solution)/shard_map/reduce_scatter | solution.py:65
Sparse Core Ops, SparseCore 0:
  23.4 49.4 all-gather.2
  85.6 67.4 reduce-scatter.2
  156.8 19.0 reduce-scatter.4
where the time goes:
time: 184 us
  waiting for transfers between devices  99.9 us (54%)
  blocking collectives  45.8 us (25%)
  matrix products  18.3 us (10%)
  between operations  13.1 us (7%)
  other arithmetic  4.99 us (3%)
    reduce_scatter x1, waiting for transfers between devices, gathered_experts(): lax.psum_scatter(jnp.sum(weight_block.T[:, :, None] * result, axis=0).ast...  64.6 us
    all_gather x1, blocking collectives, gathered_experts(): all_weights = lax.all_gather(by_expert, 'ep', axis=0, tiled=True)  31.2 us
    reduce_scatter x1, waiting for transfers between devices, body(): lax.psum_scatter((routed + shared_part).astype(jnp.bfloat16), 'tp', scatt...  19.2 us
    all_gather x1, waiting for transfers between devices, gathered_experts(): gathered_rows = lax.all_gather(source_rows, 'ep', axis=0, tiled=True)  16 us
    dot_general x1, matrix products, gathered_experts(): jnp.einsum('erf,efd->erd', inner_value, down_proj, preferred_element_type...  8.62 us
    psum x1, blocking collectives, body(): squares = lax.psum(jnp.sum(values * values, axis=1), 'tp')  8.4 us
    all_gather x1, blocking collectives, body(): full_rows = lax.all_gather(normed, 'tp', axis=1, tiled=True)  6.23 us
    dot_general x1, matrix products, gathered_experts(): jnp.einsum('rd,edf->erf', all_rows, gate_proj, preferred_element_type=jnp...  4.06 us
  transfers between devices with their start and end apart: 3, of which 3 were waited for; matrix products, arithmetic and copies ran while one was open for 2% of the time, Pallas kernels for 0%

commit v1 on v0

v1 whole, which is shorter than its diff:
```python
import functools

import jax
import jax.numpy as jnp
from jax import lax
from jax.experimental import pallas as pl
from jax.experimental.pallas import tpu as pltpu
from jax.sharding import PartitionSpec as P

epsilon = 1e-06
MESH = pl.DeviceIdType.MESH
F32 = jnp.float32
BF16 = jnp.bfloat16


def factors(ep, tp):
    x_size = 1
    while x_size * x_size * 4 <= ep and ep % (x_size * 2) == 0:
        x_size *= 2
    return x_size, ep // x_size, tp // 2


def kernel(
    ep, tp, hid, gain, wsend, wg_h, wu_h, wd_h, sg_h, su_h, sd_h, out,
    wg, wu, wd, sg, su, gath, xg, gains, wrecv, ss, acc_g, acc_u, sacc_g, sacc_u, inner,
    part, from_core, from_diag, from_x, from_y, from_z,
    local_sem, send_sem, gat_sem, sib_sem, gain_sem, w_sem, core_sem, diag_sem, x_sem, y_sem, z_sem,
):
    X, Z, Y = factors(ep, tp)
    S, Dt = hid.shape
    LE, D, F = wg.shape
    SF = sg.shape[1]
    R = ep * S
    ZS = Z * S
    half = Z // 2
    me_e, me_t = lax.axis_index("ep"), lax.axis_index("tp")
    z, x = me_e // X, me_e % X
    y, c = me_t // 2, me_t % 2

    def loc(dx=0, dy=0, dz=0, dc=0):
        return ((z + dz) % Z) * X + (x + dx) % X, ((y + dy) % Y) * 2 + (c + dc) % 2

    copies = []

    def load(src, dst):
        copy = pltpu.make_async_copy(src, dst, local_sem.at[len(copies)])
        copy.start()
        copies.append(copy)

    load(wg_h, wg)
    load(wu_h, wu)
    load(sg_h, sg)
    load(su_h, su)
    for e in range(LE):
        load(wd_h.at[e], wd.at[pl.ds(e * F, F)])
    load(sd_h, wd.at[pl.ds(LE * F, SF)])

    barrier = pltpu.get_barrier_semaphore()
    for de in range(1, ep):
        pl.semaphore_signal(barrier, inc=1, device_id=((me_e + de) % ep, me_t), device_id_type=MESH)
    for dt in range(1, tp):
        pl.semaphore_signal(barrier, inc=1, device_id=(me_e, (me_t + dt) % tp), device_id_type=MESH)
    pl.semaphore_wait(barrier, ep + tp - 2)

    sends = []

    def send(src, dst, rsem, device):
        copy = pltpu.make_async_remote_copy(
            src_ref=src, dst_ref=dst, send_sem=send_sem.at[len(sends)], recv_sem=rsem,
            device_id=device, device_id_type=MESH)
        copy.start()
        sends.append(copy)

    def arrived(dst, rsem):
        pltpu.make_async_remote_copy(
            src_ref=dst, dst_ref=dst, send_sem=send_sem.at[0], recv_sem=rsem,
            device_id=loc(dc=1), device_id_type=MESH).wait_recv()

    def row_of(xx, zz):
        return pl.multiple_of((xx * Z + zz) * S, S)

    def block(dx, dy, dz, dc=0):
        t = ((y - dy + Y) % Y) * 2 + (c + dc) % 2
        return gath.at[t, pl.ds(row_of((x - dx + X) % X, (z - dz + Z) % Z), S)]

    def slot(dx, dy, dz):
        return (dx * Y + dy) * Z + dz

    def pass_on(dx, dy, dz):
        own = dx == 0 and dy == 0 and dz == 0
        here = block(dx, dy, dz)
        if own:
            src = hid
        else:
            arrived(here, gat_sem.at[slot(dx, dy, dz)])
            src = here
        if own:
            for k in sorted(range(1, Z), key=lambda k: min(k, Z - k)):
                send(src, here, gat_sem.at[slot(0, 0, k)], loc(dz=k))
        if dx == 0 and (dy == 0 or dz >= half):
            for k in range(1, X):
                send(src, here, gat_sem.at[slot(k, dy, dz)], loc(dx=k))
        if dy == 0 and (dx == 0 or dz < half):
            for k in range(1, Y):
                send(src, here, gat_sem.at[slot(dx, k, dz)], loc(dy=k))
        send(src, here, sib_sem.at[slot(dx, dy, dz)], loc(dc=1))

    pass_on(0, 0, 0)
    for dt in range(1, tp):
        send(gain, gains.at[me_t], gain_sem.at[dt], (me_e, (me_t + dt) % tp))
    for de in range(1, ep):
        to = (me_e + de) % ep
        send(wsend.at[to], wrecv.at[me_e], w_sem.at[de], (to, me_t))
    gath[me_t, pl.ds(row_of(x, z), S)] = hid[...]
    gains[me_t] = gain[...]
    wrecv[me_e] = wsend[me_e]
    inner[:, LE * F:] = jnp.zeros((R, SF), BF16)
    ss[...] = jnp.zeros_like(ss)

    def line(dz):
        for dx in range(1, X):
            pass_on(dx, 0, dz)
        for dy in range(1, Y):
            pass_on(0, dy, dz)

    previous = 0
    for dz in sorted(range(1, Z), key=lambda k: min(k, Z - k)):
        pass_on(0, 0, dz)
        line(previous)
        previous = dz
    line(previous)
    for dt in range(1, tp):
        arrived(gains.at[(me_t + tp - dt) % tp], gain_sem.at[dt])
    waited = [False]

    rows_tile = min(R, 256)

    def project(dy, dc, first):
        t = ((y - dy + Y) % Y) * 2 + (c + dc) % 2

        def scale_rows(i, carry):
            rows = pl.ds(pl.multiple_of(i * S, S), S)
            values = gath[t, rows, :].astype(F32)
            squares = values * values
            total = squares[:, :128]
            for k in range(1, Dt // 128):
                total += squares[:, k * 128:(k + 1) * 128]
            ss[rows, :] += total
            xg[rows, :] = (values * gains[t]).astype(BF16)
            return carry

        lax.fori_loop(0, ep, scale_rows, 0)
        if not waited[0]:
            for k in range(4):
                copies[k].wait()
            waited[0] = True
        depth = pl.ds(pl.multiple_of(t * Dt, Dt), Dt)

        def experts(i, carry):
            e = i // (R // rows_tile)
            rows = pl.ds(pl.multiple_of((i % (R // rows_tile)) * rows_tile, rows_tile), rows_tile)
            g = jnp.dot(xg[rows, :], wg[e, depth, :], preferred_element_type=F32)
            u = jnp.dot(xg[rows, :], wu[e, depth, :], preferred_element_type=F32)
            if first:
                acc_g[e, rows, :] = g
                acc_u[e, rows, :] = u
            else:
                acc_g[e, rows, :] += g
                acc_u[e, rows, :] += u
            return carry

        lax.fori_loop(0, LE * (R // rows_tile), experts, 0)
        mine = xg[pl.ds(row_of(x, z), S), :]
        g = jnp.dot(mine, sg[depth, :], preferred_element_type=F32)
        u = jnp.dot(mine, su[depth, :], preferred_element_type=F32)
        if first:
            sacc_g[...] = g
            sacc_u[...] = u
        else:
            sacc_g[...] += g
            sacc_u[...] += u

    def from_sibling(dy):
        for dx in range(X):
            for dz in range(Z):
                arrived(block(dx, dy, dz, 1), sib_sem.at[slot(dx, dy, dz)])

    project(0, 0, True)
    for dz in range(Z):
        for dx in range(1, X):
            for dy in range(1, Y):
                pass_on(dx, dy, dz)
    from_sibling(0)
    project(0, 1, False)
    for dy in range(1, Y):
        project(dy, 0, False)
        from_sibling(dy)
        project(dy, 1, False)

    for de in range(1, ep):
        arrived(wrecv.at[(me_e + ep - de) % ep], w_sem.at[de])

    def scale_of(rows):
        return lax.rsqrt(jnp.sum(ss[rows, :], axis=1, keepdims=True) / D + epsilon)

    def gated(g, u):
        return g / (1.0 + jnp.exp(-g)) * u

    lanes = lax.broadcasted_iota(jnp.int32, (S, 128), 1)
    diagonal = lanes == lax.broadcasted_iota(jnp.int32, (S, 128), 0)

    def finish(i, carry):
        rows = pl.ds(pl.multiple_of(i * S, S), S)
        scale = scale_of(rows)
        weights = wrecv[(i % Z) * X + i // Z]
        for e in range(LE):
            column = jnp.sum(jnp.where(diagonal, weights[e:e + 1, :], 0.0), axis=1, keepdims=True)
            value = gated(acc_g[e, rows, :] * scale, acc_u[e, rows, :] * scale) * column
            inner[rows, e * F:(e + 1) * F] = value.astype(BF16)
        return carry

    lax.fori_loop(0, ep, finish, 0)
    own_rows = pl.ds(row_of(x, z), S)
    own_scale = scale_of(own_rows)
    inner[own_rows, LE * F:] = gated(sacc_g[...] * own_scale, sacc_u[...] * own_scale).astype(BF16)
    for copy in copies[4:]:
        copy.wait()

    tile = min(Dt, 256)

    def down(dx, dy, dc):
        rows = pl.ds(pl.multiple_of(((x + dx) % X) * ZS, ZS), ZS)
        t = ((y + dy) % Y) * 2 + (c + dc) % 2
        K = LE * F + (SF if dx == 0 else 0)

        def columns(n, carry):
            cols = pl.ds(pl.multiple_of(n * tile, tile), tile)
            wide = pl.ds(pl.multiple_of(t * Dt + n * tile, tile), tile)
            value = jnp.dot(inner[rows, :K], wd[:K, wide], preferred_element_type=F32)
            part[t, rows, cols] = value.astype(BF16)
            return carry

        lax.fori_loop(0, Dt // tile, columns, 0)

    def t_of(dy, dc=0):
        return ((y + dy) % Y) * 2 + (c + dc) % 2

    def line_rows(dx):
        return pl.ds(pl.multiple_of(((x + dx) % X) * ZS, ZS), ZS)

    def start_chunk(dx, dy):
        down(dx, dy, 1)
        send(part.at[t_of(dy, 1), line_rows(dx)], from_core.at[dx, dy], core_sem.at[dx * Y + dy], loc(dc=1))
        down(dx, dy, 0)

    def reduce_chunk(dx, dy):
        arrived(from_core.at[dx, dy], core_sem.at[dx * Y + dy])
        order = list(range(Z))
        for k in order:
            zz = k if dx or dy else (z + (k + 1)) % Z
            rows = pl.ds(row_of((x + dx) % X, zz), S)
            core_rows = pl.ds(pl.multiple_of(zz * S, S), S)
            total = part[t_of(dy), rows, :].astype(F32) + from_core[dx, dy, core_rows, :].astype(F32)
            if dx and not dy and k < half:
                for b in range(1, Y):
                    arrived(from_diag.at[dx - 1, b - 1, k], diag_sem.at[((dx - 1) * (Y - 1) + b - 1) * Z + k])
                    total += from_diag[dx - 1, b - 1, k].astype(F32)
            if dy and not dx and k >= half:
                for a in range(1, X):
                    arrived(from_diag.at[a - 1, dy - 1, k], diag_sem.at[((a - 1) * (Y - 1) + dy - 1) * Z + k])
                    total += from_diag[a - 1, dy - 1, k].astype(F32)
            if not dx and not dy:
                if k == 0:
                    for zk in range(Z):
                        for a in range(1, X):
                            arrived(from_x.at[a - 1, zk], x_sem.at[(a - 1) * Z + zk])
                        for b in range(1, Y):
                            arrived(from_y.at[b - 1, zk], y_sem.at[(b - 1) * Z + zk])
                for a in range(1, X):
                    total += from_x[a - 1, zz].astype(F32)
                for b in range(1, Y):
                    total += from_y[b - 1, zz].astype(F32)
                if k == Z - 1:
                    for dz in range(1, Z):
                        arrived(from_z.at[dz - 1], z_sem.at[dz])
                        total += from_z[dz - 1].astype(F32)
                    out[...] = total.astype(BF16)
                    return
            part[t_of(dy), rows, :] = total.astype(BF16)
            src = part.at[t_of(dy), rows]
            if dx and dy:
                sem = diag_sem.at[((dx - 1) * (Y - 1) + dy - 1) * Z + k]
                send(src, from_diag.at[dx - 1, dy - 1, k], sem, loc(dy=dy) if k < half else loc(dx=dx))
            elif dx:
                send(src, from_x.at[dx - 1, k], x_sem.at[(dx - 1) * Z + k], loc(dx=dx))
            elif dy:
                send(src, from_y.at[dy - 1, k], y_sem.at[(dy - 1) * Z + k], loc(dy=dy))
            else:
                send(src, from_z.at[k], z_sem.at[k + 1], loc(dz=k + 1))

    chunks = [(dx, dy) for dx in range(X) for dy in range(Y)]
    chunks.sort(key=lambda p: -((p[0] > 0) + (p[1] > 0)))
    start_chunk(*chunks[0])
    for before, after in zip(chunks, chunks[1:]):
        start_chunk(*after)
        reduce_chunk(*before)
    reduce_chunk(*chunks[-1])
    for copy in sends:
        copy.wait_send()


def solution(mesh):
    ep, tp = mesh.shape["ep"], mesh.shape["tp"]
    X, Z, Y = factors(ep, tp)

    def body(hidden, norm_gain, expert_ids, route_weights, lengths, gate_proj, up_proj, down_proj,
             shared_gate, shared_up, shared_down):
        S, Dt = hidden.shape
        LE, D, F = gate_proj.shape
        SF = shared_gate.shape[1]
        R = ep * S
        span = S // lengths.shape[0]
        offsets = jnp.arange(S, dtype=jnp.int32) % span
        is_live = offsets < jnp.repeat(lengths, span)
        mixing = jnp.where(is_live[:, None], route_weights, 0.0)
        padded = -(-LE // 8) * 8
        named = jnp.arange(padded, dtype=jnp.int32)[None, :] + LE * jnp.arange(ep, dtype=jnp.int32)[:, None]
        hit = expert_ids.T[:, None, None, :] == named[None, :, :, None]
        wsend = jnp.sum(jnp.where(hit, mixing.T[:, None, None, :], 0.0), axis=0)
        wsend = jnp.pad(wsend, ((0, 0), (0, 0), (0, 128 - S)))
        blocks = X * Y * Z
        n_sends = 2 * blocks - 1 + tp - 1 + ep - 1 + X * Y + blocks - 1
        vmem = pl.BlockSpec(memory_space=pltpu.VMEM)
        hbm = pl.BlockSpec(memory_space=pl.ANY)
        dma = pltpu.SemaphoreType.DMA
        combined = pl.pallas_call(
            functools.partial(kernel, ep, tp),
            out_shape=jax.ShapeDtypeStruct((S, Dt), BF16),
            in_specs=[vmem] * 3 + [hbm] * 6,
            out_specs=vmem,
            scratch_shapes=[
                pltpu.VMEM((LE, D, F), BF16),
                pltpu.VMEM((LE, D, F), BF16),
                pltpu.VMEM((LE * F + SF, D), BF16),
                pltpu.VMEM((D, SF), BF16),
                pltpu.VMEM((D, SF), BF16),
                pltpu.VMEM((tp, R, Dt), BF16),
                pltpu.VMEM((R, Dt), BF16),
                pltpu.VMEM((tp, 1, Dt), F32),
                pltpu.VMEM((ep, padded, 128), F32),
                pltpu.VMEM((R, 128), F32),
                pltpu.VMEM((LE, R, F), F32),
                pltpu.VMEM((LE, R, F), F32),
                pltpu.VMEM((S, SF), F32),
                pltpu.VMEM((S, SF), F32),
                pltpu.VMEM((R, LE * F + SF), BF16),
                pltpu.VMEM((tp, R, Dt), BF16),
                pltpu.VMEM((X, Y, Z * S, Dt), BF16),
                pltpu.VMEM((max(X - 1, 1), max(Y - 1, 1), Z, S, Dt), BF16),
                pltpu.VMEM((max(X - 1, 1), Z, S, Dt), BF16),
                pltpu.VMEM((max(Y - 1, 1), Z, S, Dt), BF16),
                pltpu.VMEM((max(Z - 1, 1), S, Dt), BF16),
                dma((5 + LE,)),
                dma((n_sends,)),
                dma((blocks,)),
                dma((blocks,)),
                dma((tp,)),
                dma((ep,)),
                dma((X * Y,)),
                dma((max((X - 1) * (Y - 1) * Z, 1),)),
                dma((max((X - 1) * Z, 1),)),
                dma((max((Y - 1) * Z, 1),)),
                dma((Z,)),
            ],
            compiler_params=pltpu.CompilerParams(
                collective_id=0, has_side_effects=True, vmem_limit_bytes=60 * 1024 * 1024),
        )(hidden, norm_gain[None, :], wsend, gate_proj, up_proj, down_proj, shared_gate, shared_up, shared_down)
        return jnp.where(is_live[:, None], combined, jnp.zeros_like(combined))

    placed = (
        P("ep", "tp"),
        P("tp"),
        P("ep", None),
        P("ep", None),
        P("ep"),
        P("ep", None, "tp"),
        P("ep", None, "tp"),
        P("ep", "tp", None),
        P(None, "tp"),
        P(None, "tp"),
        P("tp", None),
    )
    return jax.shard_map(body, mesh=mesh, in_specs=placed, out_specs=P("ep", "tp"), check_vma=False)
```

time: 184 us -> 53.8 us (0.29)
  waiting for transfers between devices: 99.9 us -> 0 us
  Pallas kernels: 0 us -> 48.9 us
  blocking collectives: 45.8 us -> 0 us
  matrix products: 18.3 us -> 0 us
  between operations: 13.1 us -> 0.01 us
  other arithmetic: 4.99 us -> 3.12 us
    reduce_scatter x2 -> x0, waiting for transfers between devices: 83.8 us -> none  [the longest x1 64.6 us: gathered_experts(): lax.psum_scatter(jnp.sum(weight_block.T[:, :, None] * result, axis=0).ast...]
    pallas_call x0 -> x1, Pallas kernels: none -> 48.9 us  [body(): pl.pallas_call(functools.partial(kernel, ep, tp), out_shape=jax.ShapeDtyp...]
    all_gather x2 -> x0, blocking collectives: 37.4 us -> none  [the longest x1 31.2 us: gathered_experts(): all_weights = lax.all_gather(by_expert, 'ep', axis=0, tiled=True)]
    dot_general x4 -> x0, matrix products: 18.3 us -> none  [the longest x1 8.62 us: gathered_experts(): jnp.einsum('erf,efd->erd', inner_value, down_proj, preferred_element_type...]
    all_gather x1 -> x0, waiting for transfers between devices: 16 us -> none  [gathered_experts(): gathered_rows = lax.all_gather(source_rows, 'ep', axis=0, tiled=True)]
    psum x1 -> x0, blocking collectives: 8.4 us -> none  [body(): squares = lax.psum(jnp.sum(values * values, axis=1), 'tp')]
    convert_element_type x2 -> x0, other arithmetic: 2.47 us -> none  [the longest x1 1.55 us: body(): return jnp.where(is_live[:, None], combined, 0.0).astype(jnp.bfloat16)]
  transfers between devices with their start and end apart: 3 -> 0, of which waited for: 3 -> 0; matrix products, arithmetic and copies ran while one was open for 2% -> 0% of each run, Pallas kernels for 0% -> 0%
where the time goes in v1:
time: 53.8 us; the launch traced here: 53.5 us
  Pallas kernels  48.9 us (91%)
  other arithmetic  3.12 us (6%)
  local copies, waits for them, and re-layouts  1.43 us (3%)
    pallas_call x1, Pallas kernels, body(): pl.pallas_call(functools.partial(kernel, ep, tp), out_shape=jax.ShapeDtyp...  48.9 us
    select_n x1, other arithmetic, body(): return jnp.where(is_live[:, None], combined, jnp.zeros_like(combined))  1.55 us

profile of v1, /device:TPU:0, one launch (start us, length us, event | category | flops | bytes accessed | tf_op | source)
XLA Modules:
  0.0 53.5 jit_solution(8221928495195650749)
XLA Ops:
  0.0 0.7 %broadcast_in_dim.48 = s32[4,8]{1,0:T(4,128)S(1)} broadcast(s32[4]{0:T(128)} %param.15), dimensions={0} | broadcast | bytes 144 | tf_op jit(solution)/shard_map/broadcast_in_dim | solution.py:324
  0.7 0.1 reshape.46
  0.8 0.1 iota_add_fusion
  0.9 0.7 %select_bitcast_fusion = f32[8,32]{1,0:T(8,128)S(1)} fusion(f32[32,8]{0,1:T(8,128)} %param.14, pred[32]{0:T(512)(128)(4,1)S(1)} %fusion), kind=kLoop, calls=%fused_computation.2 | loop fusion | flops 256 | bytes 2080 | tf_op jit(solution)/shard_map/transpose | solution.py:329
  1.6 0.8 %select_reduce_fusion = f32[8,8,32]{2,1,0:T(8,128)S(1)} fusion(f32[8,32]{1,0:T(8,128)S(1)} %select_bitcast_fusion, s32[8,8]{1,0:T(8,128)S(1)} %iota_add_fusion, s32[8,32]{1,0:T(8,128)} %bitcast.4), kind=kLoop, calls=%fused_computation | loop fusion | flops 47104 | bytes 10496 | tf_op jit(solution)/shard_map/reduce_sum | solution.py:329
  2.4 0.6 %pad.4.wsend = f32[8,8,128]{2,1,0:T(8,128)} pad(f32[8,8,32]{2,1,0:T(8,128)S(1)} %select_reduce_fusion, f32[]{:T(128)} %constant.22.clone.1), padding=0_0x0_0x0_96 | pad | bytes 40964 | tf_op jit(solution)/shard_map/jit(_pad)/pad | solution.py:330
  3.0 48.9 %shard_map.109 = bf16[32,1024]{1,0:T(8,128)(2,1)} custom-call(bf16[32,1024]{1,0:T(8,128)(2,1)} %hid.1, f32[1,1024]{1,0:T(1,128)} %bitcast.5, f32[8,8,128]{2,1,0:T(8,128)} %pad.4.wsend, bf16[2,4096,256]{2,1,0:T(8,128)(2,1)} %wg_h.1, bf16[2,4096,256]{2,1,0:T(8,128)(2,1)} %wu_h.1, bf16[2,256,4096]{2,1,0:T(8,128)(2,1)} %wd_h.1, bf16[4096,256]{1,0:T(8,128)(2,1)} %sg_h.1, ...), custom_call_target="tpu_custom_call" | custom-call | tf_op jit(solution)/shard_map/pallas_call | solution.py:336
  52.0 1.5 %broadcast_select_fusion = bf16[32,1024]{1,0:T(8,128)(2,1)} fusion(bf16[32,1024]{1,0:T(8,128)(2,1)} %shard_map.109, pred[32]{0:T(512)(128)(4,1)S(1)} %fusion), kind=kLoop, calls=%fused_computation.1 | loop fusion | flops 32768 | bytes 131104 | tf_op jit(solution)/shard_map/jit(_where)/select_n | solution.py:378
  (2 shorter events, 0.0 us)

commit v2 on v1

--- a/solution.py
+++ b/solution.py
@@ -21,8 +21,8 @@
 
 
 def kernel(
-    ep, tp, hid, gain, wsend, wg_h, wu_h, wd_h, sg_h, su_h, sd_h, out,
-    wg, wu, wd, sg, su, gath, xg, gains, wrecv, ss, acc_g, acc_u, sacc_g, sacc_u, inner,
+    ep, tp, hid, gain, ids, mix, lengths, wg_h, wu_h, wd_h, sg_h, su_h, sd_h, out,
+    wg, wu, wd, sg, su, gath, xg, gains, wsend, wrecv, ss, acc_g, acc_u, sacc_g, sacc_u, inner,
     part, from_core, from_diag, from_x, from_y, from_z,
     local_sem, send_sem, gat_sem, sib_sem, gain_sem, w_sem, core_sem, diag_sem, x_sem, y_sem, z_sem,
 ):
@@ -32,7 +32,8 @@
     SF = sg.shape[1]
     R = ep * S
     ZS = Z * S
-    half = Z // 2
+    near = sorted(range(1, Z), key=lambda k: min(k, Z - k))
+    first_x = [k for p, k in enumerate([0] + near) if p % 2 == 0]
     me_e, me_t = lax.axis_index("ep"), lax.axis_index("tp")
     z, x = me_e // X, me_e % X
     y, c = me_t // 2, me_t % 2
@@ -95,12 +96,12 @@
             arrived(here, gat_sem.at[slot(dx, dy, dz)])
             src = here
         if own:
-            for k in sorted(range(1, Z), key=lambda k: min(k, Z - k)):
+            for k in near:
                 send(src, here, gat_sem.at[slot(0, 0, k)], loc(dz=k))
-        if dx == 0 and (dy == 0 or dz >= half):
+        if dx == 0 and (dy == 0 or dz not in first_x):
             for k in range(1, X):
                 send(src, here, gat_sem.at[slot(k, dy, dz)], loc(dx=k))
-        if dy == 0 and (dx == 0 or dz < half):
+        if dy == 0 and (dx == 0 or dz in first_x):
             for k in range(1, Y):
                 send(src, here, gat_sem.at[slot(dx, k, dz)], loc(dy=k))
         send(src, here, sib_sem.at[slot(dx, dy, dz)], loc(dc=1))
@@ -108,6 +109,22 @@
     pass_on(0, 0, 0)
     for dt in range(1, tp):
         send(gain, gains.at[me_t], gain_sem.at[dt], (me_e, (me_t + dt) % tp))
+    span = S // lengths.shape[0]
+    position = lax.broadcasted_iota(jnp.int32, (1, S), 1)
+    limit = jnp.zeros((1, S), jnp.int32)
+    for q in range(lengths.shape[0]):
+        limit = jnp.where(position // span == q, lengths[q], limit)
+    mixing = jnp.where(position % span < limit, mix[...], 0.0)
+    named = ids[...]
+    wsend[...] = jnp.zeros_like(wsend)
+
+    def weights_for(j, carry):
+        for e in range(LE):
+            hit = named == j * LE + e
+            wsend[j, e:e + 1, :S] = jnp.sum(jnp.where(hit, mixing, 0.0), axis=0, keepdims=True)
+        return carry
+
+    lax.fori_loop(0, ep, weights_for, 0)
     for de in range(1, ep):
         to = (me_e + de) % ep
         send(wsend.at[to], wrecv.at[me_e], w_sem.at[de], (to, me_t))
@@ -124,7 +141,7 @@
             pass_on(0, dy, dz)
 
     previous = 0
-    for dz in sorted(range(1, Z), key=lambda k: min(k, Z - k)):
+    for dz in near:
         pass_on(0, 0, dz)
         line(previous)
         previous = dz
@@ -186,7 +203,7 @@
                 arrived(block(dx, dy, dz, 1), sib_sem.at[slot(dx, dy, dz)])
 
     project(0, 0, True)
-    for dz in range(Z):
+    for dz in [0] + near:
         for dx in range(1, X):
             for dy in range(1, Y):
                 pass_on(dx, dy, dz)
@@ -226,7 +243,7 @@
     for copy in copies[4:]:
         copy.wait()
 
-    tile = min(Dt, 256)
+    tile = min(Dt, 512)
 
     def down(dx, dy, dc):
         rows = pl.ds(pl.multiple_of(((x + dx) % X) * ZS, ZS), ZS)
@@ -253,58 +270,82 @@
         send(part.at[t_of(dy, 1), line_rows(dx)], from_core.at[dx, dy], core_sem.at[dx * Y + dy], loc(dc=1))
         down(dx, dy, 0)
 
-    def reduce_chunk(dx, dy):
+    order = near + [0]
+
+    def diag_slot(dx, dy, p):
+        return ((dx - 1) * (Y - 1) + dy - 1) * Z + p
+
+    def reduce_block(dx, dy, p):
+        zz = (z + order[p]) % Z
+        rows = pl.ds(row_of((x + dx) % X, zz), S)
+        core_rows = pl.ds(pl.multiple_of(zz * S, S), S)
+        total = part[t_of(dy), rows, :].astype(F32) + from_core[dx, dy, core_rows, :].astype(F32)
+        if dx and not dy and p % 2 == 1:
+            for b in range(1, Y):
+                arrived(from_diag.at[dx - 1, b - 1, p], diag_sem.at[diag_slot(dx, b, p)])
+                total += from_diag[dx - 1, b - 1, p].astype(F32)
+        if dy and not dx and p % 2 == 0:
+            for a in range(1, X):
+                arrived(from_diag.at[a - 1, dy - 1, p], diag_sem.at[diag_slot(a, dy, p)])
+                total += from_diag[a - 1, dy - 1, p].astype(F32)
+        if not dx and not dy:
+            for a in range(1, X):
+                arrived(from_x.at[a - 1, p], x_sem.at[(a - 1) * Z + p])
+                total += from_x[a - 1, p].astype(F32)
+            for b in range(1, Y):
+                arrived(from_y.at[b - 1, p], y_sem.at[(b - 1) * Z + p])
+                total += from_y[b - 1, p].astype(F32)
+            if p == Z - 1:
+                for dz in near:
+                    arrived(from_z.at[dz - 1], z_sem.at[dz])
+                    total += from_z[dz - 1].astype(F32)
+                out[...] = total.astype(BF16)
+                return
+        part[t_of(dy), rows, :] = total.astype(BF16)
+        src = part.at[t_of(dy), rows]
+        if dx and dy:
+            sem = diag_sem.at[diag_slot(dx, dy, p)]
+            send(src, from_diag.at[dx - 1, dy - 1, p], sem, loc(dx=dx) if p % 2 == 0 else loc(dy=dy))
+        elif dx:
+            send(src, from_x.at[dx - 1, p], x_sem.at[(dx - 1) * Z + p], loc(dx=dx))
+        elif dy:
+            send(src, from_y.at[dy - 1, p], y_sem.at[(dy - 1) * Z + p], loc(dy=dy))
+        else:
+            dz = order[p]
+            send(src, from_z.at[dz - 1], z_sem.at[dz], loc(dz=dz))
+
+    def core_arrived(dx, dy):
         arrived(from_core.at[dx, dy], core_sem.at[dx * Y + dy])
-        order = list(range(Z))
-        for k in order:
-            zz = k if dx or dy else (z + (k + 1)) % Z
-            rows = pl.ds(row_of((x + dx) % X, zz), S)
-            core_rows = pl.ds(pl.multiple_of(zz * S, S), S)
-            total = part[t_of(dy), rows, :].astype(F32) + from_core[dx, dy, core_rows, :].astype(F32)
-            if dx and not dy and k < half:
-                for b in range(1, Y):
-                    arrived(from_diag.at[dx - 1, b - 1, k], diag_sem.at[((dx - 1) * (Y - 1) + b - 1) * Z + k])
-                    total += from_diag[dx - 1, b - 1, k].astype(F32)
-            if dy and not dx and k >= half:
-                for a in range(1, X):
-                    arrived(from_diag.at[a - 1, dy - 1, k], diag_sem.at[((a - 1) * (Y - 1) + dy - 1) * Z + k])
-                    total += from_diag[a - 1, dy - 1, k].astype(F32)
-            if not dx and not dy:
-                if k == 0:
-                    for zk in range(Z):
-                        for a in range(1, X):
-                            arrived(from_x.at[a - 1, zk], x_sem.at[(a - 1) * Z + zk])
-                        for b in range(1, Y):
-                            arrived(from_y.at[b - 1, zk], y_sem.at[(b - 1) * Z + zk])
-                for a in range(1, X):
-                    total += from_x[a - 1, zz].astype(F32)
-                for b in range(1, Y):
-                    total += from_y[b - 1, zz].astype(F32)
-                if k == Z - 1:
-                    for dz in range(1, Z):
-                        arrived(from_z.at[dz - 1], z_sem.at[dz])
-                        total += from_z[dz - 1].astype(F32)
-                    out[...] = total.astype(BF16)
-                    return
-            part[t_of(dy), rows, :] = total.astype(BF16)
-            src = part.at[t_of(dy), rows]
-            if dx and dy:
-                sem = diag_sem.at[((dx - 1) * (Y - 1) + dy - 1) * Z + k]
-                send(src, from_diag.at[dx - 1, dy - 1, k], sem, loc(dy=dy) if k < half else loc(dx=dx))
-            elif dx:
-                send(src, from_x.at[dx - 1, k], x_sem.at[(dx - 1) * Z + k], loc(dx=dx))
-            elif dy:
-                send(src, from_y.at[dy - 1, k], y_sem.at[(dy - 1) * Z + k], loc(dy=dy))
-            else:
-                send(src, from_z.at[k], z_sem.at[k + 1], loc(dz=k + 1))
-
-    chunks = [(dx, dy) for dx in range(X) for dy in range(Y)]
-    chunks.sort(key=lambda p: -((p[0] > 0) + (p[1] > 0)))
-    start_chunk(*chunks[0])
-    for before, after in zip(chunks, chunks[1:]):
-        start_chunk(*after)
-        reduce_chunk(*before)
-    reduce_chunk(*chunks[-1])
+
+    far = [(dx, dy) for dx in range(1, X) for dy in range(1, Y)]
+    sides_x = [(dx, 0) for dx in range(1, X)]
+    sides_y = [(0, dy) for dy in range(1, Y)]
+    for pair in far:
+        start_chunk(*pair)
+    for pair in sides_x:
+        start_chunk(*pair)
+    for pair in far:
+        core_arrived(*pair)
+    for p in range(Z):
+        for pair in far:
+            reduce_block(*pair, p)
+    for pair in sides_y:
+        start_chunk(*pair)
+    for pair in sides_x + sides_y:
+        core_arrived(*pair)
+    y_order = list(range(Z))
+    for p in range(0, Z - 1, 2):
+        y_order[p], y_order[p + 1] = p + 1, p
+    for i in range(Z):
+        for pair in sides_x:
+            reduce_block(*pair, i)
+        for pair in sides_y:
+            reduce_block(*pair, y_order[i])
+        if i == 0:
+            start_chunk(0, 0)
+    core_arrived(0, 0)
+    for p in range(Z):
+        reduce_block(0, 0, p)
     for copy in sends:
         copy.wait_send()
 
@@ -322,12 +363,7 @@
         span = S // lengths.shape[0]
         offsets = jnp.arange(S, dtype=jnp.int32) % span
         is_live = offsets < jnp.repeat(lengths, span)
-        mixing = jnp.where(is_live[:, None], route_weights, 0.0)
         padded = -(-LE // 8) * 8
-        named = jnp.arange(padded, dtype=jnp.int32)[None, :] + LE * jnp.arange(ep, dtype=jnp.int32)[:, None]
-        hit = expert_ids.T[:, None, None, :] == named[None, :, :, None]
-        wsend = jnp.sum(jnp.where(hit, mixing.T[:, None, None, :], 0.0), axis=0)
-        wsend = jnp.pad(wsend, ((0, 0), (0, 0), (0, 128 - S)))
         blocks = X * Y * Z
         n_sends = 2 * blocks - 1 + tp - 1 + ep - 1 + X * Y + blocks - 1
         vmem = pl.BlockSpec(memory_space=pltpu.VMEM)
@@ -336,7 +372,7 @@
         combined = pl.pallas_call(
             functools.partial(kernel, ep, tp),
             out_shape=jax.ShapeDtypeStruct((S, Dt), BF16),
-            in_specs=[vmem] * 3 + [hbm] * 6,
+            in_specs=[vmem] * 4 + [pl.BlockSpec(memory_space=pltpu.SMEM)] + [hbm] * 6,
             out_specs=vmem,
             scratch_shapes=[
                 pltpu.VMEM((LE, D, F), BF16),
@@ -347,6 +383,7 @@
                 pltpu.VMEM((tp, R, Dt), BF16),
                 pltpu.VMEM((R, Dt), BF16),
                 pltpu.VMEM((tp, 1, Dt), F32),
+                pltpu.VMEM((ep, padded, 128), F32),
                 pltpu.VMEM((ep, padded, 128), F32),
                 pltpu.VMEM((R, 128), F32),
                 pltpu.VMEM((LE, R, F), F32),
@@ -374,7 +411,8 @@
             ],
             compiler_params=pltpu.CompilerParams(
                 collective_id=0, has_side_effects=True, vmem_limit_bytes=60 * 1024 * 1024),
-        )(hidden, norm_gain[None, :], wsend, gate_proj, up_proj, down_proj, shared_gate, shared_up, shared_down)
+        )(hidden, norm_gain[None, :], expert_ids.T, route_weights.T, lengths, gate_proj, up_proj, down_proj,
+          shared_gate, shared_up, shared_down)
         return jnp.where(is_live[:, None], combined, jnp.zeros_like(combined))
 
     placed = (

time: 53.8 us -> 49.7 us (0.924)
  Pallas kernels: 48.9 us -> 47.1 us
  other arithmetic: 3.12 us -> 1.56 us
  local copies, waits for them, and re-layouts: 1.43 us -> 0.81 us
    pallas_call x1, Pallas kernels: 48.9 us -> 47.1 us  [body(): pl.pallas_call(functools.partial(kernel, ep, tp), out_shape=jax.ShapeDtyp...]
    reduce_sum x1 -> x0, other arithmetic: 0.79 us -> none  [body(): wsend = jnp.sum(jnp.where(hit, mixing.T[:, None, None, :], 0.0), axis=0)]
    transpose x1 -> x0, other arithmetic: 0.69 us -> none  [body(): wsend = jnp.sum(jnp.where(hit, mixing.T[:, None, None, :], 0.0), axis=0)]
    pad x1 -> x0, local copies, waits for them, and re-layouts: 0.62 us -> none  [body(): wsend = jnp.pad(wsend, ((0, 0), (0, 0), (0, 128 - S)))]
where the time goes in v2:
time: 49.7 us; the launch traced here: 49.4 us
  Pallas kernels  47.1 us (95%)
  other arithmetic  1.56 us (3%)
  local copies, waits for them, and re-layouts  0.81 us (2%)
    pallas_call x1, Pallas kernels, body(): pl.pallas_call(functools.partial(kernel, ep, tp), out_shape=jax.ShapeDtyp...  47.1 us
    select_n x1, other arithmetic, body(): return jnp.where(is_live[:, None], combined, jnp.zeros_like(combined))  1.55 us

profile of v2, /device:TPU:0, one launch (start us, length us, event | category | flops | bytes accessed | tf_op | source)
XLA Modules:
  0.0 49.4 jit_solution(10412611943506487212)
XLA Ops:
  0.0 0.7 %broadcast_in_dim.18 = s32[4,8]{1,0:T(4,128)S(1)} broadcast(s32[4]{0:T(128)} %lengths.1), dimensions={0} | broadcast | bytes 144 | tf_op jit(solution)/shard_map/broadcast_in_dim | solution.py:365
  0.7 0.1 reshape.17
  0.8 47.1 %shard_map.109 = bf16[32,1024]{1,0:T(8,128)(2,1)} custom-call(bf16[32,1024]{1,0:T(8,128)(2,1)} %hid.1, f32[1,1024]{1,0:T(1,128)} %bitcast.3, s32[8,32]{1,0:T(8,128)} %bitcast.4, f32[8,32]{1,0:T(8,128)} %bitcast.5, s32[4]{0:T(128)} %lengths.1, bf16[2,4096,256]{2,1,0:T(8,128)(2,1)} %wg_h.1, bf16[2,4096,256]{2,1,0:T(8,128)(2,1)} %wu_h.1, ...), custom_call_target="tpu_custom_call" | custom-call | tf_op jit(solution)/shard_map/pallas_call | solution.py:372
  47.9 1.5 %broadcast_select_fusion = bf16[32,1024]{1,0:T(8,128)(2,1)} fusion(bf16[32,1024]{1,0:T(8,128)(2,1)} %shard_map.109, pred[32]{0:T(512)(128)(4,1)S(1)} %fusion), kind=kLoop, calls=%fused_computation | loop fusion | flops 32768 | bytes 131104 | tf_op jit(solution)/shard_map/jit(_where)/select_n | solution.py:416
  (1 shorter events, 0.0 us)
